TPU v7x, 512 devices: a whole 4x4x16 slice. The times are simulated.
512 devices in a mesh: ep: 32 (over z, core), tp: 16 (over y, x).
Axes of the slice: x: 4, y: 4, z: 16, core: 2. Of those that a mesh axis runs over, the one named last changes fastest.
Arguments:
- tokens: bfloat16 [1024, 2048], P('ep', 'tp'), may hold values from -200 to 200
- routing: int32 [1024, 4], P('ep'), may hold values from 0 to 63, all different within a row; in each aligned block of 32 rows (0 to 31, 32 to 63, ...) at most 8 rows name the same one
- gate_weights: float32 [1024, 4], P('ep'), may hold values from 0.05 to 1
- norm_gain: float32 [2048], replicated, may hold values from 0.1 to 1.9
- w_gate: bfloat16 [64, 2048, 2048], P('ep', None, 'tp'), may hold values from -0.33007812 to 0.33007812
- w_up: bfloat16 [64, 2048, 2048], P('ep', None, 'tp'), may hold values from -0.33007812 to 0.33007812
- w_down: bfloat16 [64, 2048, 2048], P('ep', 'tp'), may hold values from -0.026489258 to 0.026489258
Outputs:
- mixed: bfloat16 [1024, 2048], P('ep', 'tp')
Inputs may be any that keep to these rules, and one draw needn't show every extreme that they name: `routing`: each token names 4 different experts. Among the 32 tokens of one index of ep no expert is named more than 8 times, a bound that some block reaches.
All inputs are finite; a program needn't handle non-finite values.
Results may differ from a plain program's by a relative error of at most 0.015.
Values may be sent and summed in bfloat16 or wider, within the bound.
No kernel may reach another device: no remote copies, remote signals or barrier semaphores. Data moves between devices by JAX's collectives and lax.ppermute only.
A program may use at most 128 MiB of HBM per device.

v0:
```python
import functools

import jax
import jax.numpy as jnp
from jax import lax
from jax.sharding import Mesh
from jax.sharding import PartitionSpec as P

D = 2048
CAP = 8
TP = ("tp_0", "tp_1")


norm_eps = 1e-06
clamp_limit = 7.0
swish_alpha = 1.702


def one_axis_at_a_time(array, axes):
    return functools.reduce(lax.psum, axes, array)


def sent_to_all(array, axis):
    copies = jnp.broadcast_to(array, (lax.axis_size(axis), *array.shape))
    return lax.all_to_all(copies, axis, split_axis=0, concat_axis=0, tiled=True)


def in_order(pieces, dim):
    pieces = jnp.moveaxis(pieces, 0, dim)
    shape = pieces.shape
    return pieces.reshape(*shape[:dim], shape[dim] * shape[dim + 1], *shape[dim + 2 :])


def gathered_copies(array, axis, dim):
    pieces = sent_to_all(array, axis)
    return in_order(pieces, dim)


def in_blocks(array, dim, length):
    shape = array.shape
    pieces = array.reshape(*shape[:dim], length, shape[dim] // length, *shape[dim + 1 :])
    return jnp.moveaxis(pieces, dim, 0)


def summed_on_arrival(array, axis, dim):
    pieces = in_blocks(array, dim, lax.axis_size(axis))
    arrived = lax.all_to_all(pieces, axis, split_axis=0, concat_axis=0, tiled=True)
    return arrived.astype(jnp.float32).sum(axis=0)


def activate(pre_gate, pre_up):
    clamped = jnp.minimum(pre_gate, clamp_limit)
    upper = jnp.clip(pre_up, -clamp_limit, clamp_limit)
    return (clamped * jax.nn.sigmoid(swish_alpha * clamped) * (upper + 1.0)).astype(jnp.bfloat16)


def per_device(tokens, routing, gate_weights, norm_gain, w_gate, w_up, w_down):
    ep_size = lax.axis_size("ep")
    exp_here = w_gate.shape[0]
    expert_count = exp_here * ep_size
    tok_rows = tokens.shape[0]
    top_count = routing.shape[1]
    col_width = tokens.shape[1]
    chosen = routing.reshape(-1)
    onehot = (chosen[:, None] == jnp.arange(expert_count, dtype=jnp.int32)[None, :]).astype(
        jnp.int32
    )
    slot_rank = jnp.sum(jnp.cumsum(onehot, axis=0) * onehot, axis=1) - 1
    slot_index = (chosen * CAP + slot_rank).reshape(tok_rows, top_count)
    slot_ids = jnp.arange(expert_count * CAP, dtype=jnp.int32)
    matches = slot_ids[:, None, None] == slot_index[None, :, :]
    placing = jnp.sum(matches.astype(jnp.float32), axis=2).astype(jnp.bfloat16)
    wide = tokens.astype(jnp.float32)
    ssq = one_axis_at_a_time(jnp.sum(wide * wide, axis=1), TP)
    gain_cols = lax.dynamic_slice_in_dim(norm_gain, lax.axis_index(TP) * col_width, col_width)
    normed = (wide * lax.rsqrt(ssq / D + norm_eps)[:, None] * gain_cols[None, :]).astype(
        jnp.bfloat16
    )
    outgoing = jnp.dot(placing, normed, preferred_element_type=jnp.float32).astype(jnp.bfloat16)
    outgoing = outgoing.reshape(ep_size, exp_here, CAP, col_width)
    received = lax.all_to_all(outgoing, "ep", split_axis=0, concat_axis=0, tiled=True)
    block_cols = gathered_copies(received, TP, 3)
    gate_part = jnp.einsum("secd,edf->secf", block_cols, w_gate, preferred_element_type=jnp.float32)
    up_part = jnp.einsum("secd,edf->secf", block_cols, w_up, preferred_element_type=jnp.float32)
    hidden = activate(gate_part, up_part)
    partial_value = jnp.einsum("secf,efd->secd", hidden, w_down, preferred_element_type=jnp.float32)
    summed = summed_on_arrival(partial_value.astype(jnp.bfloat16), TP, 3).astype(jnp.bfloat16)
    returned = lax.all_to_all(summed, "ep", split_axis=0, concat_axis=0, tiled=True)
    returned = returned.reshape(expert_count * CAP, col_width).astype(jnp.float32)
    combine = jnp.sum(matches.astype(jnp.float32) * gate_weights[None, :, :], axis=2)
    mixed = jnp.dot(combine.T, returned, precision=lax.Precision.HIGHEST)
    return mixed.astype(jnp.bfloat16)


def solution(mesh):
    split = Mesh(mesh.devices.reshape(mesh.shape["ep"], 4, 4), ("ep", "tp_0", "tp_1"))
    placed = (
        P("ep", TP),
        P("ep", None),
        P("ep", None),
        P(),
        P("ep", None, TP),
        P("ep", None, TP),
        P("ep", TP, None),
    )
    return jax.shard_map(
        per_device, mesh=split, in_specs=placed, out_specs=P("ep", TP), check_vma=False
    )
```

profile of v0, /device:TPU:1, one launch (start us, length us, event | category | flops | bytes accessed | tf_op | source)
XLA Modules:
  0.0 149.6 jit_solution(17330649923930033378)
XLA Ops:
  0.0 0.0 copy-start
  0.0 0.9 fusion.48
  0.9 9.5 %psum.14 = f32[32]{0:T(128)S(1)} all-reduce(f32[32]{0:T(128)S(1)} %fusion.48), channel_id=1, replica_groups=mesh['ep'=32,'tp_0'=4,'tp_1'=4] {'tp_0'}, use_global_device_ids=true, to_apply=%region_5.6 | all-reduce | flops 32 | bytes 256 | tf_op jit(solution)/shard_map/psum | solution.py:20
  10.4 8.5 %psum.15 = f32[32]{0:T(128)S(1)} all-reduce(f32[32]{0:T(128)S(1)} %psum.14), channel_id=1, replica_groups=mesh['ep'=32,'tp_0'=4,'tp_1'=4] {'tp_1'}, use_global_device_ids=true, to_apply=%region_6.7 | all-reduce | flops 32 | bytes 256 | tf_op jit(solution)/shard_map/psum | solution.py:20
  18.9 0.8 copy.53
  19.7 0.1 eq.29
  19.8 0.1 fusion.46
  19.9 0.2 reduce_window_sum.11
  20.0 0.2 select_reduce_fusion.1
  20.2 0.1 sub.7
  20.3 0.1 copy.54
  20.4 0.7 multiply_add_fusion
  21.1 0.8 dynamic_slice.3
  21.9 0.8 convert_reduce_fusion
  22.7 0.9 convolution_convert_fusion.1
  23.6 35.6 %all_to_all.20 = bf16[32,2,8,128]{3,2,1,0:T(8,128)(2,1)S(1)} all-to-all(bf16[32,2,8,128]{3,2,1,0:T(8,128)(2,1)S(1)} %bitcast.69), channel_id=1, replica_groups=mesh['ep'=32,'tp_0'=4,'tp_1'=4] {'ep'}, dimensions={0} | all-to-all | bytes 262144 | tf_op jit(solution)/shard_map/all_to_all | solution.py:81
  59.2 0.5 broadcast_in_dim.2
  59.7 0.0 copy-start.1
  59.7 29.9 %all_to_all.21 = bf16[16,32,2,8,128]{4,3,1,2,0:T(8,128)(2,1)S(1)} all-to-all(bf16[16,32,2,8,128]{4,3,1,2,0:T(8,128)(2,1)S(1)} %broadcast_in_dim.2), channel_id=1, replica_groups=mesh['ep'=32,'tp_0'=4,'tp_1'=4] {'tp_0','tp_1'}, dimensions={0} | all-to-all | bytes 4194304 | tf_op jit(solution)/shard_map/all_to_all | solution.py:25
  89.6 0.0 copy-done.1
  89.6 0.7 fusion.10
  90.3 0.0 copy-done
  90.3 3.9 %fusion.6 = bf16[32,2,8,16,128]{4,2,3,0,1:T(8,128)(2,1)} fusion(bf16[2,128,2048]{2,1,0:T(8,128)(2,1)S(1)} %copy-done, bf16[2,2048,128]{2,1,0:T(8,128)(2,1)} %param.12, f32[32,2,8,128]{3,2,0,1:T(8,128)S(1)} %fusion.10, bf16[16,32,2,8,128]{4,3,1,2,0:T(8,128)(2,1)S(1)} %all_to_all.21), kind=kOutput, calls=%fused_computation.8 | convolution fusion | flops 538509312 | bytes 6553600 | tf_op jit(solution)/shard_map/secf,efd->secd/dot_general | solution.py:86
  94.2 2.2 %copy.89 = bf16[32,2,8,16,128]{4,2,0,1,3:T(8,128)(2,1)S(1)} copy(bf16[32,2,8,16,128]{4,2,3,0,1:T(8,128)(2,1)} %fusion.6) | data formatting | bytes 4194304 | tf_op jit(solution)/shard_map/reshape | solution.py:41
  96.4 30.1 %all_to_all.22 = bf16[16,32,2,8,128]{4,3,1,2,0:T(8,128)(2,1)S(1)} all-to-all(bf16[16,32,2,8,128]{4,3,1,2,0:T(8,128)(2,1)S(1)} %bitcast.68), channel_id=1, replica_groups=mesh['ep'=32,'tp_0'=4,'tp_1'=4] {'tp_0','tp_1'}, dimensions={0} | all-to-all | bytes 4194304 | tf_op jit(solution)/shard_map/all_to_all | solution.py:47
  126.5 0.3 reduce_sum.52
  126.8 22.0 %all_to_all.23 = bf16[32,2,8,128]{3,2,1,0:T(8,128)(2,1)S(1)} all-to-all(bf16[32,2,8,128]{3,2,1,0:T(8,128)(2,1)S(1)} %copy.59), channel_id=1, replica_groups=mesh['ep'=32,'tp_0'=4,'tp_1'=4] {'ep'}, dimensions={0} | all-to-all | bytes 262144 | tf_op jit(solution)/shard_map/all_to_all | solution.py:88
  148.8 0.8 convolution_convert_fusion.2
  (4 shorter events, 0.0 us)
Async XLA Ops:
  0.0 90.3 %copy-start = (bf16[2,128,2048]{2,1,0:T(8,128)(2,1)S(1)}, bf16[2,128,2048]{2,1,0:T(8,128)(2,1)}, u32[]{:S(2)}) copy-start(bf16[2,128,2048]{2,1,0:T(8,128)(2,1)} %param.13) | copy-start | bytes 3145732
  59.7 29.9 %copy-start.1 = (bf16[2,2048,128]{2,1,0:T(8,128)(2,1)S(1)}, bf16[2,2048,128]{2,1,0:T(8,128)(2,1)}, u32[]{:S(2)}) copy-start(bf16[2,2048,128]{2,1,0:T(8,128)(2,1)} %param.11) | copy-start | bytes 3145732
where the time goes:
time: 150 us
  blocking collectives  136 us (91%)
  matrix products  6.35 us (4%)
  local copies, waits for them, and re-layouts  4.48 us (3%)
  other arithmetic  3.12 us (2%)
    all_to_all x1, blocking collectives, per_device(): lax.all_to_all(outgoing, 'ep', split_axis=0, concat_axis=0, tiled=True)  35.6 us
    all_to_all x1, blocking collectives, summed_on_arrival(): lax.all_to_all(pieces, axis, split_axis=0, concat_axis=0, tiled=True)  30.1 us
    all_to_all x1, blocking collectives, sent_to_all(): return lax.all_to_all(copies, axis, split_axis=0, concat_axis=0, tiled=True)  29.9 us
    all_to_all x1, blocking collectives, per_device(): lax.all_to_all(summed, 'ep', split_axis=0, concat_axis=0, tiled=True)  22 us
    psum x2, blocking collectives, one_axis_at_a_time(): return functools.reduce(lax.psum, axes, array)  18 us
    dot_general x1, matrix products, per_device(): jnp.einsum('secf,efd->secd', hidden, w_down, preferred_element_type=jnp.f...  3.92 us

commit v1 on v0

v1 whole, which is shorter than its diff:
```python
import functools

import jax
import jax.numpy as jnp
from jax import lax
from jax.experimental import pallas as pl
from jax.experimental.pallas import tpu as pltpu
from jax.sharding import Mesh
from jax.sharding import PartitionSpec as P

D = 2048
CAP = 8
TP = ("tp_0", "tp_1")
BUCKETS = (512,)

norm_eps = 1e-06
clamp_limit = 7.0
swish_alpha = 1.702
EMPTY = 512.0
FILLED_BELOW = 256.0

f32 = jnp.float32
bf16 = jnp.bfloat16
VMEM = pl.BlockSpec(memory_space=pltpu.VMEM)
SMEM = pl.BlockSpec(memory_space=pltpu.SMEM)
ANY = pl.BlockSpec(memory_space=pl.ANY)


def iota(shape, dim):
    return lax.broadcasted_iota(jnp.int32, shape, dim)


def dot(a, b):
    return jnp.dot(a, b, preferred_element_type=f32)


def dispatch_kernel(routing_ref, weight_ref, tokens_ref, out_ref, high_ref, low_ref):
    slots = out_ref.shape[0]
    top, rows = routing_ref.shape
    slot = iota((slots, rows), 0)
    expert = slot // CAP
    chosen = jnp.zeros((slots, rows), f32)
    weight = jnp.zeros((slots, rows), f32)
    for k in range(top):
        match = routing_ref[k : k + 1, :] == expert
        chosen = jnp.where(match, 1.0, chosen)
        weight = jnp.where(match, weight_ref[k : k + 1, :], weight)
    before = (iota((rows, rows), 0) < iota((rows, rows), 1)).astype(f32).astype(bf16)
    rank = dot(chosen.astype(bf16), before).astype(jnp.int32)
    placed = jnp.where(rank == slot % CAP, chosen, 0.0)
    placing = placed.astype(bf16)
    rows_out = dot(placing, tokens_ref[...])
    filled = dot(placing, jnp.ones((rows, out_ref.shape[1]), bf16))
    out_ref[...] = jnp.where(filled > 0.5, rows_out, EMPTY).astype(bf16)
    weight = weight * placed
    high = weight.astype(bf16)
    high_ref[...] = high
    low_ref[...] = (weight - high.astype(f32)).astype(bf16)


def dispatch(routing, gate_weights, tokens, slots):
    top, rows = routing.shape
    return pl.pallas_call(
        dispatch_kernel,
        out_shape=(
            jax.ShapeDtypeStruct((slots, tokens.shape[1]), bf16),
            jax.ShapeDtypeStruct((slots, rows), bf16),
            jax.ShapeDtypeStruct((slots, rows), bf16),
        ),
        in_specs=[VMEM] * 3,
        out_specs=(VMEM,) * 3,
        name="dispatch",
    )(routing, gate_weights, tokens)


def order_key(index):
    local = (index // CAP) % 2
    source = index // (2 * CAP)
    return local * 4096 + source * CAP + index % CAP


def order_kernel(received_ref, column_ref, row_ref, count_ref):
    slots, width = received_ref.shape
    filled = received_ref[...].astype(f32) < FILLED_BELOW
    ones = jnp.where(filled, 1.0, 0.0).astype(bf16)
    key_0 = order_key(iota((slots, slots), 0))
    key_1 = order_key(iota((slots, slots), 1))
    column = dot((key_1 < key_0).astype(f32).astype(bf16), ones)
    column = jnp.where(filled, column, -1.0)
    column_ref[...] = column
    across = lax.dot_general(
        jnp.ones((8, width), bf16), ones, (((1,), (1,)), ((), ())), preferred_element_type=f32
    )
    across = jnp.where(across > 0.5, 1.0, 0.0)
    row = dot(across.astype(bf16), (key_0 < key_1).astype(f32).astype(bf16))
    row = jnp.where(across > 0.5, row, -1.0)
    row_ref[...] = row
    total = jnp.max(row).astype(jnp.int32) + 1
    is_first = (iota((8, slots), 1) // CAP) % 2 == 0
    first = jnp.max(jnp.where(is_first, row, -1.0)).astype(jnp.int32) + 1
    bucket = jnp.int32(0)
    for size in BUCKETS[:-1]:
        bucket = bucket + (total > size).astype(jnp.int32)
    count_ref[0] = first
    count_ref[1] = bucket


def order_rows(received):
    slots, width = received.shape
    return pl.pallas_call(
        order_kernel,
        out_shape=(
            jax.ShapeDtypeStruct((slots, width), f32),
            jax.ShapeDtypeStruct((8, slots), f32),
            jax.ShapeDtypeStruct((2,), jnp.int32),
        ),
        in_specs=[VMEM],
        out_specs=(VMEM, VMEM, SMEM),
        name="order_rows",
    )(received)


def compact_kernel(received_ref, row_ref, out_ref):
    copies, size, _ = out_ref.shape
    slots = received_ref.shape[0]
    position = iota((size, slots), 0).astype(f32)
    pick = jnp.where(row_ref[0:1, :] == position, 1.0, 0.0).astype(bf16)
    rows = dot(pick, received_ref[...]).astype(bf16)
    for n in range(copies):
        out_ref[n] = rows


def compact(received, row, copies, size):
    return pl.pallas_call(
        compact_kernel,
        out_shape=jax.ShapeDtypeStruct((copies, size, received.shape[1]), bf16),
        in_specs=[VMEM] * 2,
        out_specs=VMEM,
        name="compact",
    )(received, row)


def expert_kernel(
    count_ref, x_ref, gain_ref, gate_ref, up_ref, down_ref, out_ref, wide, narrow, normed, sems
):
    parts, size, width = x_ref.shape
    copies = []
    for e in range(2):
        for m, ref in enumerate((gate_ref, up_ref)):
            at = (2 * e + m) * width
            copies.append(
                pltpu.make_async_copy(ref.at[e], wide.at[:, at : at + width], sems.at[2 * e + m])
            )
    copies.append(pltpu.make_async_copy(down_ref, narrow, sems.at[4]))
    for copy in copies:
        copy.start()
    ssq = jnp.zeros((size, width), f32)
    for p in range(parts):
        x = x_ref[p].astype(f32)
        ssq = ssq + x * x
    scale = lax.rsqrt(jnp.sum(ssq, axis=1, keepdims=True) / D + norm_eps)
    for p in range(parts):
        x = x_ref[p].astype(f32) * scale * gain_ref[p : p + 1, :]
        normed[:, p * width : (p + 1) * width] = x.astype(bf16)
    for copy in copies[:4]:
        copy.wait()
    pre = dot(normed[...], wide[...])
    row = iota((size, width), 0)
    first = count_ref[0]
    hidden = []
    for e in range(2):
        clamped = jnp.minimum(pre[:, 2 * e * width : (2 * e + 1) * width], clamp_limit)
        upper = jnp.clip(pre[:, (2 * e + 1) * width : (2 * e + 2) * width], -clamp_limit, clamp_limit)
        value = clamped * jax.nn.sigmoid(swish_alpha * clamped) * (upper + 1.0)
        mine = row < first if e == 0 else row >= first
        hidden.append(jnp.where(mine, value, 0.0).astype(bf16))
    hidden = jnp.concatenate(hidden, axis=1)
    copies[4].wait()
    for p in range(0, parts, 2):
        out = dot(hidden, narrow[:, p * width : (p + 2) * width]).astype(bf16)
        out_ref[p] = out[:, :width]
        out_ref[p + 1] = out[:, width:]


def experts(count, x, gain, gate, up, down):
    parts, size, width = x.shape
    return pl.pallas_call(
        expert_kernel,
        out_shape=jax.ShapeDtypeStruct(x.shape, bf16),
        in_specs=[SMEM, VMEM, VMEM, ANY, ANY, ANY],
        out_specs=VMEM,
        scratch_shapes=[
            pltpu.VMEM((D, 4 * width), bf16),
            pltpu.VMEM((2 * width, D), bf16),
            pltpu.VMEM((size, D), bf16),
            pltpu.SemaphoreType.DMA((5,)),
        ],
        name="experts",
    )(count, x, gain, gate, up, down)


def expand_kernel(parts_ref, column_ref, out_ref, total):
    parts, size, width = parts_ref.shape
    slots = column_ref.shape[0]
    padded = total.shape[0]
    value = parts_ref[0].astype(f32)
    for p in range(1, parts):
        value = value + parts_ref[p].astype(f32)
    if padded > size:
        total[...] = jnp.zeros(total.shape, bf16)
    total[:size, :] = value.astype(bf16)
    column = column_ref[...]
    lane = iota((slots, width), 1).astype(f32)
    picks = [
        jnp.where(column == lane + float(b * width), 1.0, 0.0).astype(bf16)
        for b in range(padded // width)
    ]
    out_ref[...] = dot(jnp.concatenate(picks, axis=1), total[...]).astype(bf16)


def expand(parts, column):
    _, size, width = parts.shape
    padded = -(-size // width) * width
    return pl.pallas_call(
        expand_kernel,
        out_shape=jax.ShapeDtypeStruct((column.shape[0], width), bf16),
        in_specs=[VMEM] * 2,
        out_specs=VMEM,
        scratch_shapes=[pltpu.VMEM((padded, width), bf16)],
        name="expand",
    )(parts, column)


def combine_kernel(returned_ref, high_ref, low_ref, out_ref):
    contract = (((0,), (0,)), ((), ()))
    returned = returned_ref[...]
    mixed = lax.dot_general(high_ref[...], returned, contract, preferred_element_type=f32)
    mixed = mixed + lax.dot_general(low_ref[...], returned, contract, preferred_element_type=f32)
    out_ref[...] = mixed.astype(bf16)


def combine(returned, high, low):
    return pl.pallas_call(
        combine_kernel,
        out_shape=jax.ShapeDtypeStruct((high.shape[1], returned.shape[1]), bf16),
        in_specs=[VMEM] * 3,
        out_specs=VMEM,
        name="combine",
    )(returned, high, low)


def exchange(pieces, axis):
    return lax.all_to_all(pieces, axis, split_axis=0, concat_axis=0, tiled=True)


def per_device(tokens, routing, gate_weights, norm_gain, w_gate, w_up, w_down):
    ep_size = lax.axis_size("ep")
    tp_size = lax.axis_size(TP)
    exp_here = w_gate.shape[0]
    width = tokens.shape[1]
    slots = ep_size * exp_here * CAP
    gain = norm_gain.reshape(tp_size, width)
    down = w_down.reshape(exp_here * w_down.shape[1], w_down.shape[2])
    outgoing, high, low = dispatch(routing.T, gate_weights.T, tokens, slots)
    received = exchange(outgoing.reshape(ep_size, exp_here * CAP, width), "ep")
    received = received.reshape(slots, width)
    column, row, count = order_rows(received)

    def middle(size, received, column, row, count, gain, w_gate, w_up, down):
        rows = exchange(compact(received, row, tp_size, size), TP)
        partial_value = experts(count, rows, gain, w_gate, w_up, down)
        return expand(exchange(partial_value, TP), column)

    branches = [functools.partial(middle, size) for size in BUCKETS]
    operands = (received, column, row, count, gain, w_gate, w_up, down)
    if len(branches) == 1:
        back = branches[0](*operands)
    else:
        back = lax.switch(count[1], branches, *operands)
    returned = exchange(back.reshape(ep_size, exp_here * CAP, width), "ep")
    return combine(returned.reshape(slots, width), high, low)


def solution(mesh):
    split = Mesh(mesh.devices.reshape(mesh.shape["ep"], 4, 4), ("ep", "tp_0", "tp_1"))
    placed = (
        P("ep", TP),
        P("ep", None),
        P("ep", None),
        P(),
        P("ep", None, TP),
        P("ep", None, TP),
        P("ep", TP, None),
    )
    return jax.shard_map(
        per_device, mesh=split, in_specs=placed, out_specs=P("ep", TP), check_vma=False
    )
```

time: 150 us -> 141 us (0.940)
  Pallas kernels: 0 us -> 17.7 us
  blocking collectives: 136 us -> 122 us
  matrix products: 6.35 us -> 0 us
  local copies, waits for them, and re-layouts: 4.48 us -> 0 us
  other arithmetic: 3.12 us -> 0 us
    psum x2 -> x0, blocking collectives: 18 us -> none  [one_axis_at_a_time(): return functools.reduce(lax.psum, axes, array)]
    pallas_call x0 -> x6, Pallas kernels: none -> 17.7 us  [the longest x1 6.51 us: experts(): pl.pallas_call(expert_kernel, out_shape=jax.ShapeDtypeStruct(x.shape, bf1...]
    dot_general x4 -> x0, matrix products: 6.35 us -> none  [the longest x1 3.92 us: per_device(): jnp.einsum('secf,efd->secd', hidden, w_down, preferred_element_type=jnp.f...]
    all_to_all x4, blocking collectives: 118 us -> 122 us  [exchange(): return lax.all_to_all(pieces, axis, split_axis=0, concat_axis=0, tiled=True)]
    reshape x1 -> x0, local copies, waits for them, and re-layouts: 2.16 us -> none  [in_blocks(): array.reshape(*shape[:dim], length, shape[dim] // length, *shape[dim + 1:])]
    reduce_sum x4 -> x0, other arithmetic: 2.15 us -> none  [the longest x1 0.89 us: per_device(): ssq = one_axis_at_a_time(jnp.sum(wide * wide, axis=1), TP)]
where the time goes in v1:
time: 141 us; the launch traced here: 140 us
  blocking collectives  122 us (87%)
  Pallas kernels  17.7 us (13%)
    all_to_all x4, blocking collectives, exchange(): return lax.all_to_all(pieces, axis, split_axis=0, concat_axis=0, tiled=True)  122 us
    pallas_call x1, Pallas kernels, experts(): pl.pallas_call(expert_kernel, out_shape=jax.ShapeDtypeStruct(x.shape, bf1...  6.51 us
    pallas_call x1, Pallas kernels, expand(): pl.pallas_call(expand_kernel, out_shape=jax.ShapeDtypeStruct((column.shap...  2.84 us

profile of v1, /device:TPU:1, one launch (start us, length us, event | category | flops | bytes accessed | tf_op | source)
XLA Modules:
  0.0 140.0 jit_solution(17588048068224993560)
XLA Ops:
  0.0 1.8 %dispatch.1 = (bf16[512,128]{1,0:T(8,128)(2,1)}, bf16[512,32]{1,0:T(8,128)(2,1)}, bf16[512,32]{1,0:T(8,128)(2,1)}) custom-call(s32[4,32]{1,0:T(4,128)} %bitcast.15, f32[4,32]{1,0:T(4,128)} %bitcast.16, bf16[32,128]{1,0:T(8,128)(2,1)} %tokens_ref.1), custom_call_target="tpu_custom_call" | custom-call | tf_op jit(solution)/shard_map/dispatch/pallas_call | solution.py:63
  1.8 32.7 %all_to_all.20 = bf16[32,16,128]{2,1,0:T(8,128)(2,1)} all-to-all(bf16[32,16,128]{2,1,0:T(8,128)(2,1)} %bitcast.13), channel_id=1, replica_groups=mesh['ep'=32,'tp_0'=4,'tp_1'=4] {'ep'}, dimensions={0} | all-to-all | bytes 262144 | tf_op jit(solution)/shard_map/all_to_all | solution.py:253
  34.5 2.0 %order_rows.1 = (f32[512,128]{1,0:T(8,128)}, f32[8,512]{1,0:T(8,128)}, s32[2]{0:T(128)}) custom-call(bf16[512,128]{1,0:T(8,128)(2,1)} %bitcast.8), custom_call_target="tpu_custom_call" | custom-call | tf_op jit(solution)/shard_map/order_rows/pallas_call | solution.py:110
  36.5 2.6 %compact.1 = bf16[16,512,128]{2,1,0:T(8,128)(2,1)} custom-call(bf16[512,128]{1,0:T(8,128)(2,1)} %bitcast.9, f32[8,512]{1,0:T(8,128)} %get-tuple-element.13.row_ref), custom_call_target="tpu_custom_call" | custom-call | tf_op jit(solution)/shard_map/compact/pallas_call | solution.py:134
  39.2 33.7 %all_to_all.21.x_ref = bf16[16,512,128]{2,1,0:T(8,128)(2,1)} all-to-all(bf16[16,512,128]{2,1,0:T(8,128)(2,1)} %compact.1), channel_id=1, replica_groups=mesh['ep'=32,'tp_0'=4,'tp_1'=4] {'tp_0','tp_1'}, dimensions={0} | all-to-all | bytes 4194304 | tf_op jit(solution)/shard_map/all_to_all | solution.py:253
  72.9 6.5 %experts.1 = bf16[16,512,128]{2,1,0:T(8,128)(2,1)} custom-call(s32[2]{0:T(128)} %get-tuple-element.12.count_ref, bf16[16,512,128]{2,1,0:T(8,128)(2,1)} %all_to_all.21.x_ref, f32[16,128]{1,0:T(8,128)} %bitcast.14, bf16[2,2048,128]{2,1,0:T(8,128)(2,1)} %gate_ref.1, bf16[2,2048,128]{2,1,0:T(8,128)(2,1)} %up_ref.1, bf16[256,2048]{1,0:T(8,128)(2,1)} %bitcast.10), custom_call_target="tpu_custom_call" | custom-call | tf_op jit(solution)/shard_map/experts/pallas_call | solution.py:187
  79.4 30.4 %all_to_all.22.parts_ref = bf16[16,512,128]{2,1,0:T(8,128)(2,1)} all-to-all(bf16[16,512,128]{2,1,0:T(8,128)(2,1)} %experts.1), channel_id=1, replica_groups=mesh['ep'=32,'tp_0'=4,'tp_1'=4] {'tp_0','tp_1'}, dimensions={0} | all-to-all | bytes 4194304 | tf_op jit(solution)/shard_map/all_to_all | solution.py:253
  109.8 2.8 %expand.1 = bf16[512,128]{1,0:T(8,128)(2,1)} custom-call(bf16[16,512,128]{2,1,0:T(8,128)(2,1)} %all_to_all.22.parts_ref, f32[512,128]{1,0:T(8,128)} %get-tuple-element.14.column_ref), custom_call_target="tpu_custom_call" | custom-call | tf_op jit(solution)/shard_map/expand/pallas_call | solution.py:224
  112.7 25.5 %all_to_all.23 = bf16[32,16,128]{2,1,0:T(8,128)(2,1)} all-to-all(bf16[32,16,128]{2,1,0:T(8,128)(2,1)} %bitcast.12), channel_id=1, replica_groups=mesh['ep'=32,'tp_0'=4,'tp_1'=4] {'ep'}, dimensions={0} | all-to-all | bytes 262144 | tf_op jit(solution)/shard_map/all_to_all | solution.py:253
  138.2 1.9 %combine.1 = bf16[32,128]{1,0:T(8,128)(2,1)} custom-call(bf16[512,128]{1,0:T(8,128)(2,1)} %bitcast.11, bf16[512,32]{1,0:T(8,128)(2,1)} %get-tuple-element.15.high_ref, bf16[512,32]{1,0:T(8,128)(2,1)} %get-tuple-element.16.low_ref), custom_call_target="tpu_custom_call" | custom-call | tf_op jit(solution)/shard_map/combine/pallas_call | solution.py:243

commit v2 on v1

--- a/solution.py
+++ b/solution.py
@@ -11,7 +11,7 @@
 D = 2048
 CAP = 8
 TP = ("tp_0", "tp_1")
-BUCKETS = (512,)
+BUCKETS = (144, 208, 272, 352, 416, 512)
 
 norm_eps = 1e-06
 clamp_limit = 7.0
@@ -70,6 +70,7 @@
         in_specs=[VMEM] * 3,
         out_specs=(VMEM,) * 3,
         name="dispatch",
+        compiler_params=pltpu.CompilerParams(vmem_limit_bytes=8 << 20),
     )(routing, gate_weights, tokens)
 
 
@@ -117,6 +118,7 @@
         in_specs=[VMEM],
         out_specs=(VMEM, VMEM, SMEM),
         name="order_rows",
+        compiler_params=pltpu.CompilerParams(vmem_limit_bytes=12 << 20),
     )(received)
 
 
@@ -137,6 +139,7 @@
         in_specs=[VMEM] * 2,
         out_specs=VMEM,
         name="compact",
+        compiler_params=pltpu.CompilerParams(vmem_limit_bytes=12 << 20),
     )(received, row)
 
 
@@ -196,6 +199,7 @@
             pltpu.SemaphoreType.DMA((5,)),
         ],
         name="experts",
+        compiler_params=pltpu.CompilerParams(vmem_limit_bytes=24 << 20),
     )(count, x, gain, gate, up, down)
 
 
@@ -228,6 +232,7 @@
         out_specs=VMEM,
         scratch_shapes=[pltpu.VMEM((padded, width), bf16)],
         name="expand",
+        compiler_params=pltpu.CompilerParams(vmem_limit_bytes=12 << 20),
     )(parts, column)
 
 
@@ -246,6 +251,7 @@
         in_specs=[VMEM] * 3,
         out_specs=VMEM,
         name="combine",
+        compiler_params=pltpu.CompilerParams(vmem_limit_bytes=8 << 20),
     )(returned, high, low)
 
 

time: 141 us -> 104 us (0.74)
  blocking collectives: 122 us -> 94.2 us
  Pallas kernels: 17.7 us -> 5.62 us
  local copies, waits for them, and re-layouts: 0 us -> 2.65 us
    all_to_all x4, blocking collectives: 122 us -> 94.2 us  [exchange(): return lax.all_to_all(pieces, axis, split_axis=0, concat_axis=0, tiled=True)]
    pallas_call x1, Pallas kernels: 6.51 us -> 2.74 us  [experts(): pl.pallas_call(expert_kernel, out_shape=jax.ShapeDtypeStruct(x.shape, bf1...]
    pallas_call x1, Pallas kernels: 2.84 us -> 0.3 us  [expand(): pl.pallas_call(expand_kernel, out_shape=jax.ShapeDtypeStruct((column.shap...]
    pallas_call x1, Pallas kernels: 2.64 us -> 0.18 us  [compact(): pl.pallas_call(compact_kernel, out_shape=jax.ShapeDtypeStruct((copies, si...]
    unnamed x0 -> x6, local copies, waits for them, and re-layouts: none -> 2.06 us
where the time goes in v2:
time: 104 us; the launch traced here: 103 us
  blocking collectives  94.2 us (91%)
  Pallas kernels  5.62 us (5%)
  local copies, waits for them, and re-layouts  2.65 us (3%)
    all_to_all x4, blocking collectives, exchange(): return lax.all_to_all(pieces, axis, split_axis=0, concat_axis=0, tiled=True)  94.2 us
    pallas_call x1, Pallas kernels, experts(): pl.pallas_call(expert_kernel, out_shape=jax.ShapeDtypeStruct(x.shape, bf1...  2.74 us

profile of v2, /device:TPU:1, one launch (start us, length us, event | category | flops | bytes accessed | tf_op | source)
XLA Modules:
  0.0 103.4 jit_solution(14978398065309751802)
XLA Ops:
  0.0 0.0 copy-start
  0.0 0.7 copy-done
  0.7 0.0 copy-start.1
  0.7 0.7 copy-done.1
  1.4 0.0 copy-start.2
  1.4 0.7 copy-done.2
  2.1 0.4 dispatch.1
  2.5 32.4 %all_to_all.70 = bf16[32,16,128]{2,1,0:T(8,128)(2,1)S(1)} all-to-all(bf16[32,16,128]{2,1,0:T(8,128)(2,1)S(1)} %bitcast.10), channel_id=1, replica_groups=mesh['ep'=32,'tp_0'=4,'tp_1'=4] {'ep'}, dimensions={0} | all-to-all | bytes 262144 | tf_op jit(solution)/shard_map/all_to_all | solution.py:259
  34.8 1.2 %order_rows.1 = (f32[512,128]{1,0:T(8,128)S(1)}, f32[8,512]{1,0:T(8,128)S(1)}, s32[2]{0:T(128)S(1)}) custom-call(bf16[512,128]{1,0:T(8,128)(2,1)S(1)} %bitcast.19), custom_call_target="tpu_custom_call" | custom-call | tf_op jit(solution)/shard_map/order_rows/pallas_call | solution.py:111
  36.0 0.6 slice.3
  37.3 33.6 %conditional.1 = (bf16[512,128]{1,0:T(8,128)(2,1)S(1)}) conditional(s32[]{:T(128)} %bitcast.4, (bf16[512,128]{1,0:T(8,128)(2,1)S(1)}, f32[8,512]{1,0:T(8,128)S(1)}, s32[2]{0:T(128)S(1)}, f32[16,128]{1,0:T(8,128)}, bf16[2,2048,128]{2,1,0:T(8,128)(2,1)}, /*index=5*/bf16[2,2048,128]{2,1,0:T(8,128)(2,1)}, ...), branch_computations={%region_0.0_spmd, %region_1.0_spmd, %region_2.0_spmd, %region_3.0_... | conditional | bytes 23101736 | solution.py:285
  37.3 0.0 copy-start.3
  37.3 0.0 copy-start.26
  37.3 0.2 compact.6
  37.5 17.2 %all_to_all.58.x_ref = bf16[16,144,128]{2,1,0:T(8,128)(2,1)S(1)} all-to-all(bf16[16,144,128]{2,1,0:T(8,128)(2,1)S(1)} %compact.6), channel_id=1, replica_groups=mesh['ep'=32,'tp_0'=4,'tp_1'=4] {'tp_0','tp_1'}, dimensions={0} | all-to-all | bytes 1179648 | tf_op jit(solution)/shard_map/cond/branch_0_fun/all_to_all | solution.py:259
  54.7 0.0 copy-done.3
  54.7 0.0 copy-done.26
  54.7 2.7 %experts.6 = bf16[16,144,128]{2,1,0:T(8,128)(2,1)S(1)} custom-call(s32[2]{0:T(128)S(1)} %get-tuple-element.96.count_ref, bf16[16,144,128]{2,1,0:T(8,128)(2,1)S(1)} %all_to_all.58.x_ref, f32[16,128]{1,0:T(8,128)S(1)} %copy-done.26, bf16[2,2048,128]{2,1,0:T(8,128)(2,1)S(1)} %copy-done.3, bf16[2,2048,128]{2,1,0:T(8,128)(2,1)} %get-tuple-element.113.up_ref, ...), custom_call_target="tpu_custom_call" | custom-call | tf_op jit(solution)/shard_map/cond/branch_0_fun/experts/pallas_call | solution.py:190
  57.5 12.8 %all_to_all.59.parts_ref = bf16[16,144,128]{2,1,0:T(8,128)(2,1)S(1)} all-to-all(bf16[16,144,128]{2,1,0:T(8,128)(2,1)S(1)} %experts.6), channel_id=1, replica_groups=mesh['ep'=32,'tp_0'=4,'tp_1'=4] {'tp_0','tp_1'}, dimensions={0} | all-to-all | bytes 1179648 | tf_op jit(solution)/shard_map/cond/branch_0_fun/all_to_all | solution.py:259
  70.3 0.3 expand.6
  70.8 31.8 %all_to_all.71 = bf16[32,16,128]{2,1,0:T(8,128)(2,1)S(1)} all-to-all(bf16[32,16,128]{2,1,0:T(8,128)(2,1)S(1)} %bitcast.26), channel_id=1, replica_groups=mesh['ep'=32,'tp_0'=4,'tp_1'=4] {'ep'}, dimensions={0} | all-to-all | bytes 262144 | tf_op jit(solution)/shard_map/all_to_all | solution.py:259
  102.6 0.8 combine.1
Async XLA Ops:
  0.0 0.7 copy-start
  0.7 0.7 copy-start.1
  1.4 0.7 copy-start.2
  37.3 17.4 %copy-start.3 = (bf16[2,2048,128]{2,1,0:T(8,128)(2,1)S(1)}, bf16[2,2048,128]{2,1,0:T(8,128)(2,1)}, u32[]{:S(2)}) copy-start(bf16[2,2048,128]{2,1,0:T(8,128)(2,1)} %get-tuple-element.112.gate_ref) | copy-start | bytes 3145732 | tf_op jit(solution)/shard_map/cond
  37.3 17.4 %copy-start.26 = (f32[16,128]{1,0:T(8,128)S(1)}, f32[16,128]{1,0:T(8,128)}, u32[]{:S(2)}) copy-start(f32[16,128]{1,0:T(8,128)} %get-tuple-element.110.gain_ref) | copy-start | bytes 24580 | tf_op jit(solution)/shard_map/cond
